TPU v7x, 32 devices: a whole 2x2x4 slice. The times are simulated.
32 devices in a mesh: ra: 4 (over z), cb: 4 (over y, x), dp: 2 (over core).
Axes of the slice: x: 2, y: 2, z: 4, core: 2. Of those that a mesh axis runs over, the one named last changes fastest.
Arguments:
- tokens: bfloat16 [3072, 4096], P('dp', 'ra'), may hold values from -20 to 20
- pre_gain: float32 [4096], P('ra'), may hold values from 0.1 to 1.9
- up_weight: bfloat16 [4096, 16384], P('ra', 'cb'), may hold values from -0.09375 to 0.09375
- up_bias: float32 [16384], P('cb'), may hold values from -4 to 4
- down_weight: bfloat16 [16384, 4096], P('cb', 'ra'), may hold values from -0.046875 to 0.046875
- post_gain: float32 [4096], P('ra'), may hold values from 0.1 to 1.9
Outputs:
- stream_out: bfloat16 [3072, 4096], P('dp', 'ra')
All inputs are finite; a program needn't handle non-finite values.
Results may differ from a plain program's by a relative error of at most 0.0051.
Values may be sent and summed in bfloat16 or wider, within the bound.
A program may use at most 128 MiB of HBM per device.

v0:
```python
import jax
import jax.numpy as jnp
from jax import lax
from jax.sharding import PartitionSpec as P

D = 4096
epsilon = 1e-06
residual_weight = 0.5


def activate(summed, inverse, offset):
    return jnp.square(jax.nn.relu(summed * inverse[:, None] + offset)).astype(jnp.bfloat16)


def body(tokens, pre_gain, up_weight, up_bias, down_weight, post_gain):
    stream = tokens.astype(jnp.float32)
    energy = jnp.sum(stream * stream, axis=1)
    scaled = (stream * pre_gain).astype(jnp.bfloat16)
    partial_value = jnp.dot(scaled, up_weight, preferred_element_type=jnp.float32)
    total = lax.psum(energy, "ra")
    share = lax.psum_scatter(partial_value, "ra", scatter_dimension=1, tiled=True)
    width = share.shape[1]
    offset = lax.dynamic_slice_in_dim(up_bias, lax.axis_index("ra") * width, width, 0)
    hidden = activate(share, lax.rsqrt(total / D + epsilon), offset)
    branch = jnp.dot(
        lax.all_gather(hidden, "ra", axis=1, tiled=True),
        down_weight,
        preferred_element_type=jnp.float32,
    )
    branch = lax.psum(branch, "cb")
    branch_energy = lax.psum(jnp.sum(branch * branch, axis=1), "ra")
    normed = branch * lax.rsqrt(branch_energy / D + epsilon)[:, None] * post_gain
    return (residual_weight * stream + normed).astype(jnp.bfloat16)


def solution(mesh):
    in_specs = (P("dp", "ra"), P("ra"), P("ra", "cb"), P("cb"), P("cb", "ra"), P("ra"))
    out_specs = P("dp", "ra")
    return jax.shard_map(body, mesh=mesh, in_specs=in_specs, out_specs=out_specs, check_vma=False)
```

profile of v0, /device:TPU:0, one launch (start us, length us, event | category | flops | bytes accessed | tf_op | source)
XLA Modules:
  0.0 853.5 jit_solution(10800701514293128842)
XLA Ops:
  6.5 0.0 reduce-scatter.2.cloned.1.call-start
  6.5 21.1 %fusion.4 = f32[1536,4096]{1,0:T(8,128)} fusion(bf16[1024,4096]{1,0:T(8,128)(2,1)} %param.8, bf16[1536,1024]{1,0:T(8,128)(2,1)} %param.6, f32[1024]{0:T(1024)} %param.7), kind=kOutput, calls=%fused_computation.9 | convolution fusion | flops 12889620480 | bytes 36704256 | tf_op jit(solution)/shard_map/dot_general | solution.py:19
  27.7 0.0 copy-start
  27.7 0.0 reduce-scatter.2.cloned.1.call-update
  27.7 0.0 all-gather.2.cloned.1.call-start
  27.8 0.8 dynamic_slice.3
  28.6 1.0 copy-done
  29.6 0.7 fusion.3
  30.3 14.3 %psum.21 = f32[1536]{0:T(1024)S(1)} all-reduce(f32[1536]{0:T(1024)S(1)} %fusion.3), channel_id=1, replica_groups=mesh['ra'=4,'cb'=4,'dp'=2] {'ra'}, use_global_device_ids=true, to_apply=%region_2.0 | all-reduce | flops 1536 | bytes 12288 | tf_op jit(solution)/shard_map/psum | solution.py:20
  44.6 400.5 %reduce-scatter.2.cloned.1.call-done = f32[1536,1024]{1,0:T(8,128)} async-done(((f32[1536,4096]{1,0:T(8,128)}), f32[1536,1024]{1,0:T(8,128)}) %reduce-scatter.2.cloned.1.call-update) | async-done | bytes 6291472 | tf_op jit(solution)/shard_map/reduce_scatter | solution.py:21
  445.2 5.4 multiply_convert_fusion
  450.6 0.0 all-gather.2.cloned.1.call-update
  450.6 0.0 all-reduce.2.cloned.1.call-start
  450.7 220.3 %all-gather.2.cloned.1.call-done = bf16[1536,4096]{1,0:T(8,128)(2,1)} async-done(((bf16[1536,1024]{1,0:T(8,128)(2,1)}), bf16[1536,4096]{1,0:T(8,128)(2,1)}) %all-gather.2.cloned.1.call-update) | async-done | bytes 12582928 | tf_op jit(solution)/shard_map/all_gather | solution.py:26
  671.0 19.5 %fusion.7 = f32[1536,1024]{1,0:T(8,128)} fusion(bf16[1536,4096]{1,0:T(8,128)(2,1)} %all-gather.2.cloned.1.call-done, bf16[4096,1024]{1,0:T(8,128)(2,1)} %param.10), kind=kOutput, calls=%fused_computation.13 | convolution fusion | flops 12884901888 | bytes 27262976 | tf_op jit(solution)/shard_map/dot_general | solution.py:25
  690.5 0.0 copy-start.1
  690.5 0.0 all-reduce.2.cloned.1.call-update
  690.5 136.5 %all-reduce.2.cloned.1.call-done = f32[1536,1024]{1,0:T(8,128)} async-done(((f32[1536,1024]{1,0:T(8,128)}), f32[1536,1024]{1,0:T(8,128)}) %all-reduce.2.cloned.1.call-update) | async-done | bytes 6291472 | tf_op jit(solution)/shard_map/psum | solution.py:30
  827.0 3.3 multiply_reduce_fusion
  830.3 11.9 %psum.23 = f32[1536]{0:T(1024)S(1)} all-reduce(f32[1536]{0:T(1024)S(1)} %multiply_reduce_fusion), channel_id=1, replica_groups=mesh['ra'=4,'cb'=4,'dp'=2] {'ra'}, use_global_device_ids=true, to_apply=%region_5.6 | all-reduce | flops 1536 | bytes 12288 | tf_op jit(solution)/shard_map/psum | solution.py:31
  842.3 0.0 copy-done.1
  842.3 4.7 fusion.1
  (2 shorter events, 0.0 us)
Async XLA Ops:
  6.5 438.6 %reduce-scatter.2.cloned.1.call-start = ((), (), s32[]{:S(2)}) async-start(), calls=%async_computation.1 | async-start | bytes 31457280 | tf_op jit(solution)/shard_map/reduce_scatter | solution.py:21
  27.7 1.9 copy-start
  27.7 643.3 %all-gather.2.cloned.1.call-start = ((), (), s32[]{:S(2)}) async-start(), calls=%async_computation.2 | async-start | bytes 15728640 | tf_op jit(solution)/shard_map/all_gather | solution.py:26
  450.6 376.4 %all-reduce.2.cloned.1.call-start = ((), (), s32[]{:S(2)}) async-start(), calls=%async_computation.3 | async-start | bytes 12582912 | tf_op jit(solution)/shard_map/psum | solution.py:30
  690.5 151.8 %copy-start.1 = (f32[1024]{0:T(1024)S(1)}, f32[1024]{0:T(1024)}, u32[]{:S(2)}) copy-start(f32[1024]{0:T(1024)} %param.11) | copy-start | bytes 12292
Sparse Core Ops, SparseCore 0:
  27.8 417.2 reduce-scatter.1
  450.7 220.2 all-gather.1
  690.6 136.3 all-reduce.1
where the time goes:
time: 854 us
  waiting for transfers between devices  757 us (89%)
  matrix products  40.6 us (5%)
  blocking collectives  26.3 us (3%)
  other arithmetic  14.1 us (2%)
  between operations  13.2 us (2%)
    reduce_scatter x1, waiting for transfers between devices, body(): lax.psum_scatter(partial_value, 'ra', scatter_dimension=1, tiled=True)  401 us
    all_gather x1, waiting for transfers between devices, body(): lax.all_gather(hidden, 'ra', axis=1, tiled=True)  220 us
    psum x1, waiting for transfers between devices, body(): branch = lax.psum(branch, 'cb')  137 us
    dot_general x1, matrix products, body(): jnp.dot(scaled, up_weight, preferred_element_type=jnp.float32)  21.1 us
    dot_general x1, matrix products, body(): jnp.dot(lax.all_gather(hidden, 'ra', axis=1, tiled=True), down_weight, pr...  19.5 us
  transfers between devices with their start and end apart: 3, of which 3 were waited for; matrix products, arithmetic and copies ran while one was open for 0% of the time, Pallas kernels for 0%

commit v1 on v0

--- a/solution.py
+++ b/solution.py
@@ -27,7 +27,9 @@
         down_weight,
         preferred_element_type=jnp.float32,
     )
-    branch = lax.psum(branch, "cb")
+    branch = branch
+    for hop in (1, 2):
+        branch = branch + lax.ppermute(branch, "cb", [(dev, dev ^ hop) for dev in range(4)])
     branch_energy = lax.psum(jnp.sum(branch * branch, axis=1), "ra")
     normed = branch * lax.rsqrt(branch_energy / D + epsilon)[:, None] * post_gain
     return (residual_weight * stream + normed).astype(jnp.bfloat16)

time: 854 us -> 1000 us (1.17)
  waiting for transfers between devices: 757 us -> 893 us
    ppermute x0 -> x2, waiting for transfers between devices: none -> 271 us  [body(): lax.ppermute(branch, 'cb', [(dev, dev ^ hop) for dev in range(4)])]
    psum x1 -> x0, waiting for transfers between devices: 137 us -> none  [body(): branch = lax.psum(branch, 'cb')]
  transfers between devices with their start and end apart: 3 -> 4, of which waited for: 3 -> 4; matrix products, arithmetic and copies ran while one was open for 0% -> 0% of each run, Pallas kernels for 0% -> 0%
where the time goes in v1:
time: 1000 us
  waiting for transfers between devices  893 us (89%)
  matrix products  38.4 us (4%)
  blocking collectives  23.2 us (2%)
  other arithmetic  20 us (2%)
  between operations  13.5 us (1%)
    reduce_scatter x1, waiting for transfers between devices, body(): lax.psum_scatter(partial_value, 'ra', scatter_dimension=1, tiled=True)  401 us
    ppermute x2, waiting for transfers between devices, body(): lax.ppermute(branch, 'cb', [(dev, dev ^ hop) for dev in range(4)])  271 us
    all_gather x1, waiting for transfers between devices, body(): lax.all_gather(hidden, 'ra', axis=1, tiled=True)  220 us
    dot_general x1, matrix products, body(): jnp.dot(scaled, up_weight, preferred_element_type=jnp.float32)  20.5 us
  transfers between devices with their start and end apart: 4, of which 4 were waited for; matrix products, arithmetic and copies ran while one was open for 0% of the time, Pallas kernels for 0%

profile of v1, /device:TPU:0, one launch (start us, length us, event | category | flops | bytes accessed | tf_op | source)
XLA Modules:
  0.0 999.7 jit_solution(1805430019566300692)
XLA Ops:
  6.5 0.0 copy-start.1
  6.5 0.0 reduce-scatter.2.cloned.1.call-start
  6.5 3.2 copy.7
  9.7 0.0 copy-done.1
  9.7 20.5 %fusion.4 = f32[1536,4096]{1,0:T(8,128)} fusion(bf16[1024,4096]{1,0:T(8,128)(2,1)} %param.8, bf16[1536,1024]{0,1:T(8,128)(2,1)S(1)} %copy.7, f32[1024]{0:T(1024)S(1)} %copy-done.1), kind=kOutput, calls=%fused_computation.9 | convolution fusion | flops 12889620480 | bytes 36704256 | tf_op jit(solution)/shard_map/dot_general | solution.py:19
  30.2 0.0 reduce-scatter.2.cloned.1.call-update
  30.2 0.0 all-gather.2.cloned.1.call-start
  30.3 0.7 dynamic_slice.3
  31.0 0.7 fusion.3
  31.6 14.4 %psum.14 = f32[1536]{0:T(1024)S(1)} all-reduce(f32[1536]{0:T(1024)S(1)} %fusion.3), channel_id=1, replica_groups=mesh['ra'=4,'cb'=4,'dp'=2] {'ra'}, use_global_device_ids=true, to_apply=%region_2.0 | all-reduce | flops 1536 | bytes 12288 | tf_op jit(solution)/shard_map/psum | solution.py:20
  46.1 401.4 %reduce-scatter.2.cloned.1.call-done = f32[1536,1024]{1,0:T(8,128)} async-done(((f32[1536,4096]{1,0:T(8,128)}), f32[1536,1024]{1,0:T(8,128)}) %reduce-scatter.2.cloned.1.call-update) | async-done | bytes 6291472 | tf_op jit(solution)/shard_map/reduce_scatter | solution.py:21
  447.5 5.4 multiply_convert_fusion
  452.9 0.0 all-gather.2.cloned.1.call-update
  452.9 220.4 %all-gather.2.cloned.1.call-done = bf16[1536,4096]{1,0:T(8,128)(2,1)} async-done(((bf16[1536,1024]{1,0:T(8,128)(2,1)}), bf16[1536,4096]{1,0:T(8,128)(2,1)}) %all-gather.2.cloned.1.call-update) | async-done | bytes 12582928 | tf_op jit(solution)/shard_map/all_gather | solution.py:26
  673.4 17.9 %fusion.7 = f32[1536,1024]{0,1:T(8,128)S(1)} fusion(bf16[1536,4096]{1,0:T(8,128)(2,1)} %all-gather.2.cloned.1.call-done, bf16[4096,1024]{1,0:T(8,128)(2,1)} %param.10), kind=kOutput, calls=%fused_computation.13 | convolution fusion | flops 12884901888 | bytes 27262976 | tf_op jit(solution)/shard_map/dot_general | solution.py:25
  691.3 1.5 collective-permute-start
  692.8 136.1 %collective-permute-done = f32[1536,1024]{0,1:T(8,128)} collective-permute-done((f32[1536,1024]{0,1:T(8,128)S(1)}, f32[1536,1024]{0,1:T(8,128)}, u32[]{:S(2)}, u32[]{:S(2)}) %collective-permute-start) | collective-permute-done | bytes 6291488 | tf_op jit(solution)/shard_map/ppermute | solution.py:32
  828.9 4.2 add.36
  833.1 0.0 copy-start
  833.1 1.5 collective-permute-start.1
  834.6 135.1 %collective-permute-done.1 = f32[1536,1024]{0,1:T(8,128)S(1)} collective-permute-done((f32[1536,1024]{0,1:T(8,128)S(1)}, f32[1536,1024]{0,1:T(8,128)S(1)}, u32[]{:S(2)}, u32[]{:S(2)}) %collective-permute-start.1) | collective-permute-done | bytes 6291488 | tf_op jit(solution)/shard_map/ppermute | solution.py:32
  969.7 4.1 multiply_reduce_fusion
  973.8 8.8 psum.15
  982.6 0.0 copy-done
  982.6 5.7 fusion.1
  988.2 4.6 copy.8
  (2 shorter events, 0.0 us)
Async XLA Ops:
  6.5 3.2 copy-start.1
  6.5 440.9 %reduce-scatter.2.cloned.1.call-start = ((), (), s32[]{:S(2)}) async-start(), calls=%async_computation.1 | async-start | bytes 31457280 | tf_op jit(solution)/shard_map/reduce_scatter | solution.py:21
  30.2 643.1 %all-gather.2.cloned.1.call-start = ((), (), s32[]{:S(2)}) async-start(), calls=%async_computation.2 | async-start | bytes 15728640 | tf_op jit(solution)/shard_map/all_gather | solution.py:26
  691.3 137.6 %collective-permute-start = (f32[1536,1024]{0,1:T(8,128)S(1)}, f32[1536,1024]{0,1:T(8,128)}, u32[]{:S(2)}, u32[]{:S(2)}) collective-permute-start(f32[1536,1024]{0,1:T(8,128)S(1)} %fusion.7), channel_id=1, source_target_pairs={{0,2},{2,0},{4,6},{6,4},{1,3},{3,1},{5,7},{7,5},{8,10},{10,8},{12,... | collective-permute-start | bytes 18874376 | tf_op jit(solution)/shard_map/ppermute | solution.py:32
  833.1 149.5 %copy-start = (f32[1024]{0:T(1024)S(1)}, f32[1024]{0:T(1024)}, u32[]{:S(2)}) copy-start(f32[1024]{0:T(1024)} %param.11) | copy-start | bytes 12292
  833.1 136.6 %collective-permute-start.1 = (f32[1536,1024]{0,1:T(8,128)S(1)}, f32[1536,1024]{0,1:T(8,128)S(1)}, u32[]{:S(2)}, u32[]{:S(2)}) collective-permute-start(f32[1536,1024]{0,1:T(8,128)S(1)} %add.36), channel_id=1, source_target_pairs={{0,4},{2,6},{4,0},{6,2},{1,5},{3,7},{5,1},{7,3},{8,12},{10,14},{12... | collective-permute-start | bytes 18874376 | tf_op jit(solution)/shard_map/ppermute | solution.py:32
Sparse Core Ops, SparseCore 0:
  30.3 417.0 reduce-scatter.1
  453.1 220.2 all-gather.1
